TPU v7x, 256 devices: a whole 4x4x8 slice. The times are simulated.
256 devices in a mesh: ep: 16 (over y, x), tp: 16 (over z, core).
Axes of the slice: x: 4, y: 4, z: 8, core: 2. Of those that a mesh axis runs over, the one named last changes fastest.
Arguments:
- mix_tokens: bfloat16 [32768, 2048], P(('ep', 'tp')), may hold values from -6 to 6
- mix_gain: bfloat16 [2048], replicated, may hold values from 0.099609375 to 1.8984375
- gate_proj: bfloat16 [2048, 1024], P(None, 'tp'), may hold values from -0.125 to 0.125
- conv_proj: bfloat16 [2048, 1024], P(None, 'tp'), may hold values from -0.125 to 0.125
- value_proj: bfloat16 [2048, 1024], P(None, 'tp'), may hold values from -0.125 to 0.125
- conv_taps: bfloat16 [3, 1024], P(None, 'tp'), may hold values from -3 to 3
- out_proj: bfloat16 [1024, 2048], P('tp'), may hold values from -0.1875 to 0.1875
- moe_tokens: bfloat16 [16384, 2048], P(('ep', 'tp')), may hold values from -6 to 6
- moe_gain: bfloat16 [2048], replicated, may hold values from 0.099609375 to 1.8984375
- expert_ids: int32 [16384, 2], P(('ep', 'tp')), may hold values from 0 to 15, all different within a row; in each aligned block of 64 rows (0 to 63, 64 to 127, ...) at most 9 rows name the same one
- expert_scores: float32 [16384, 2], P(('ep', 'tp')), may hold values from -6 to 6
- expert_gate: bfloat16 [16, 2048, 4096], P('ep', None, 'tp'), may hold values from -0.125 to 0.125
- expert_up: bfloat16 [16, 2048, 4096], P('ep', None, 'tp'), may hold values from -0.125 to 0.125
- expert_down: bfloat16 [16, 4096, 2048], P('ep', 'tp'), may hold values from -0.09375 to 0.09375
Outputs:
- mix_out: bfloat16 [32768, 2048], P(('ep', 'tp'))
- moe_out: bfloat16 [16384, 2048], P(('ep', 'tp'))
Inputs may be any that keep to these rules, and one draw needn't show every extreme that they name: `expert_ids`: each row names 2 different experts; among the rows of one device no expert is named more than 9 times.
All inputs are finite; a program needn't handle non-finite values.
Results may differ from a plain program's by a relative error of at most 0.018.
Values may be sent and summed in bfloat16 or wider, within the bound.
A program may use at most 128 MiB of HBM per device.

v0:
```python
import jax
import jax.numpy as jnp
from jax import lax
from jax.sharding import PartitionSpec as P

norm_eps = 1e-06


def from_behind(value, axis, steps):
    count = lax.axis_size(axis)
    leading, last = (max(0, -steps), min(count, count - steps))
    return lax.ppermute(value, axis, [(source, source + steps) for source in range(leading, last)])


def scaled_norm(row_data, gain_vec):
    values = row_data.astype(jnp.float32)
    inverse = lax.rsqrt(jnp.mean(values * values, axis=1, keepdims=True) + norm_eps)
    return (values * inverse * gain_vec.astype(jnp.float32)).astype(jnp.bfloat16)


def shards(
    mix_tokens,
    mix_gain,
    gate_proj,
    conv_proj,
    value_proj,
    conv_taps,
    out_proj,
    moe_tokens,
    moe_gain,
    expert_ids,
    expert_scores,
    expert_gate,
    expert_up,
    expert_down,
):
    normed = scaled_norm(mix_tokens, mix_gain)
    w_joint = jnp.concatenate([gate_proj, conv_proj, value_proj], axis=1)
    combined = jnp.dot(
        lax.all_gather(normed, "tp", axis=0, tiled=True),
        w_joint,
        preferred_element_type=jnp.float32,
    ).astype(jnp.bfloat16)
    channels = gate_proj.shape[1]
    out_gate = combined[:, :channels]
    in_gate = combined[:, channels : 2 * channels]
    values = combined[:, 2 * channels :]
    signal = (in_gate.astype(jnp.float32) * values.astype(jnp.float32)).astype(jnp.bfloat16)
    tap_count = conv_taps.shape[0]
    before = from_behind(signal[signal.shape[0] - (tap_count - 1) :], "ep", 1)
    extended = jnp.concatenate([before, signal], axis=0)
    length = signal.shape[0]
    tap_values = conv_taps.astype(jnp.float32)
    convolved = jnp.zeros((length, channels), jnp.float32)
    for offset in range(tap_count):
        convolved = (
            convolved + extended[offset : offset + length].astype(jnp.float32) * tap_values[offset]
        )
    carried = (out_gate.astype(jnp.float32) * convolved).astype(jnp.bfloat16)
    token_major = lax.all_to_all(carried, "tp", split_axis=0, concat_axis=1, tiled=True)
    mix_out = jnp.dot(
        token_major,
        lax.all_gather(out_proj, "tp", axis=0, tiled=True),
        preferred_element_type=jnp.float32,
    ).astype(jnp.bfloat16)
    moe_normed = scaled_norm(moe_tokens, moe_gain)
    experts = expert_gate.shape[0] * lax.axis_size("ep")
    row_count, top_count = expert_ids.shape
    capacity = top_count * row_count // experts + max(1, top_count * row_count // (8 * experts))
    width_model = moe_tokens.shape[1]
    flat_ids = expert_ids.reshape(-1)
    onehot = (flat_ids[:, None] == jnp.arange(experts, dtype=jnp.int32)[None, :]).astype(jnp.int32)
    slot_rank = jnp.sum((jnp.cumsum(onehot, axis=0) - onehot) * onehot, axis=1)
    slot_index = flat_ids * capacity + slot_rank
    slot_match = slot_index[:, None] == jnp.arange(experts * capacity, dtype=jnp.int32)[None, :]
    dispatch_map = jnp.any(
        slot_match.reshape(row_count, top_count, experts * capacity), axis=1
    ).astype(jnp.bfloat16)
    outgoing = lax.dot_general(
        dispatch_map, moe_normed, (((0,), (0,)), ((), ())), preferred_element_type=jnp.float32
    ).astype(jnp.bfloat16)
    arrived = lax.all_to_all(
        outgoing.reshape(experts, capacity, width_model),
        "ep",
        split_axis=0,
        concat_axis=0,
        tiled=True,
    )
    arrived_rows = arrived.reshape(-1, width_model)
    w_gate = expert_gate[0]
    w_up = expert_up[0]
    w_down = expert_down[0]
    portion = lax.all_gather(arrived_rows, "tp", axis=0, tiled=True)
    gate_value = jnp.dot(portion, w_gate, preferred_element_type=jnp.float32)
    up_value = jnp.dot(portion, w_up, preferred_element_type=jnp.float32)
    hidden = (jax.nn.silu(gate_value) * up_value).astype(jnp.bfloat16)
    summed = lax.psum_scatter(
        jnp.dot(hidden, w_down, preferred_element_type=jnp.float32).astype(jnp.bfloat16),
        "tp",
        scatter_dimension=0,
        tiled=True,
    )
    returned = lax.all_to_all(
        summed.reshape(experts, capacity, width_model),
        "ep",
        split_axis=0,
        concat_axis=0,
        tiled=True,
    )
    flat_back = returned.reshape(experts * capacity, width_model)
    picked = flat_back[slot_index].reshape(row_count, top_count, width_model)
    route_weight = jax.nn.softmax(expert_scores, axis=1)
    moe_out = jnp.sum(route_weight[:, :, None] * picked.astype(jnp.float32), axis=1).astype(
        jnp.bfloat16
    )
    return (mix_out, moe_out)


def solution(mesh):
    in_specs = (
        P(("ep", "tp"), None),
        P(),
        P(None, "tp"),
        P(None, "tp"),
        P(None, "tp"),
        P(None, "tp"),
        P("tp", None),
        P(("ep", "tp"), None),
        P(),
        P(("ep", "tp"), None),
        P(("ep", "tp"), None),
        P("ep", None, "tp"),
        P("ep", None, "tp"),
        P("ep", "tp", None),
    )
    out_specs = (P(("ep", "tp"), None), P(("ep", "tp"), None))
    return jax.shard_map(shards, mesh=mesh, in_specs=in_specs, out_specs=out_specs, check_vma=False)
```

profile of v0, /device:TPU:1, one launch (start us, length us, event | category | flops | bytes accessed | tf_op | source)
XLA Modules:
  0.0 292.0 jit_solution(8549273080741177627)
XLA Ops:
  7.2 0.0 copy-start
  7.2 0.0 all-gather.8.cloned.1.call-start
  7.2 0.8 copy.25
  8.1 0.1 eq.29
  8.2 0.1 fusion.24
  8.3 0.2 reduce_window_sum.11
  8.5 0.2 select_reduce_fusion
  8.7 0.1 reduce_sum.52
  8.8 0.1 copy.27
  8.9 0.1 fusion.23
  9.0 0.7 convert_element_type.89
  9.7 1.1 fusion.15
  10.8 1.3 convolution_convert_fusion.2
  12.2 0.2 reshape.87
  12.4 23.4 %all_to_all.29 = bf16[16,9,2048]{2,1,0:T(8,128)(2,1)S(1)} all-to-all(bf16[16,9,2048]{2,1,0:T(8,128)(2,1)S(1)} %reshape.87), channel_id=1, replica_groups=mesh['ep'=16,'tp'=16] {'ep'}, dimensions={0} | all-to-all | bytes 1179648 | tf_op jit(solution)/shard_map/all_to_all | solution.py:82
  35.8 1.1 reshape.88
  36.9 0.0 all-gather.8.cloned.1.call-update
  36.9 0.0 all-gather.4.cloned.1.call-start
  37.0 0.2 fusion.2
  37.2 1.0 fusion.4
  38.2 0.0 all-gather.4.cloned.1.call-update
  38.2 0.0 reduce-scatter.2.cloned.1.call-start
  38.3 60.5 %all-gather.8.cloned.1.call-done = bf16[2304,2048]{1,0:T(8,128)(2,1)} async-done(((bf16[144,2048]{1,0:T(8,128)(2,1)}), bf16[2304,2048]{1,0:T(8,128)(2,1)}) %all-gather.8.cloned.1.call-update) | async-done | bytes 9437200 | tf_op jit(solution)/shard_map/all_gather | solution.py:93
  98.7 7.7 %fusion.8 = f32[2304,256]{1,0:T(8,128)} fusion(bf16[2304,2048]{1,0:T(8,128)(2,1)} %all-gather.8.cloned.1.call-done, bf16[1,2048,256]{2,1,0:T(8,128)(2,1)S(1)} %copy-done.5), kind=kOutput, calls=%fused_computation.15 | convolution fusion | flops 2415919104 | bytes 12845056 | tf_op jit(solution)/shard_map/dot_general | solution.py:94
  106.5 14.9 %convolution_convert_fusion = bf16[2304,2048]{1,0:T(8,128)(2,1)} fusion(bf16[2304,2048]{1,0:T(8,128)(2,1)} %all-gather.8.cloned.1.call-done, f32[2304,256]{1,0:T(8,128)} %fusion.8, bf16[1,256,2048]{2,1,0:T(8,128)(2,1)S(1)} %copy-done, bf16[1,2048,256]{2,1,0:T(8,128)(2,1)} %param.26), kind=kOutput, calls=%fused_computation.1 | convolution fusion | flops 4840095744 | bytes 23330816 | tf_op jit(solution)/shard_map/dot_general | solution.py:98
  121.4 0.0 reduce-scatter.2.cloned.1.call-update
  121.4 0.0 all-gather.6.cloned.1.call-start
  121.5 0.5 all-gather.6.cloned.1.call-update
  122.0 0.1 copy-done.4
  122.1 33.5 %all-gather.4.cloned.1.call-done = bf16[2048,2048]{1,0:T(8,128)(2,1)} async-done(((bf16[128,2048]{1,0:T(8,128)(2,1)}), bf16[2048,2048]{1,0:T(8,128)(2,1)}) %all-gather.4.cloned.1.call-update) | async-done | bytes 8388624 | tf_op jit(solution)/shard_map/all_gather | solution.py:40
  155.6 6.3 %convolution_convert_fusion.1 = bf16[2048,192]{0,1:T(8,128)(2,1)S(1)} fusion(bf16[2048,2048]{1,0:T(8,128)(2,1)} %all-gather.4.cloned.1.call-done, bf16[2048,64]{0,1:T(8,128)(2,1)S(1)} %copy-done.6, bf16[2048,64]{0,1:T(8,128)(2,1)S(1)} %copy-done.7, bf16[2048,64]{0,1:T(8,128)(2,1)S(1)} %copy-done.8), kind=kOutput, calls=%fused_computation.4 | convolution fusion | flops 1613365248 | bytes 9961472 | tf_op jit(solution)/shard_map/dot_general | solution.py:39
  161.9 0.1 multiply_convert_fusion.1
  162.0 0.1 slice.41
  162.0 3.1 %collective-permute-start = (bf16[2,64]{0,1:T(8,128)(2,1)S(1)}, bf16[2,64]{0,1:T(8,128)(2,1)S(1)}, u32[]{:S(2)}, u32[]{:S(2)}) collective-permute-start(bf16[2,64]{0,1:T(8,128)(2,1)S(1)} %slice.41), channel_id=1, source_target_pairs={{0,16},{16,32},{32,48},{48,64},{64,80},{80,96},{96,112},{112,128},... | collective-permute-start | bytes 776 | tf_op jit(solution)/shard_map/ppermute | solution.py:12
  165.1 0.8 collective-permute-done
  166.0 1.0 copy_bitcast_fusion
  167.0 5.4 %all-to-all-start = ((bf16[16,128,64]{1,2,0:T(8,128)(2,1)}), bf16[16,128,64]{1,2,0:T(8,128)(2,1)S(1)}, u32[]{:S(2)}, u32[]{:S(2)}) async-start(bf16[16,128,64]{1,2,0:T(8,128)(2,1)} %copy_bitcast_fusion), calls=%async_computation | async-start | bytes 524288 | tf_op jit(solution)/shard_map/all_to_all | solution.py:60
  172.4 0.1 mul.138
  172.6 58.9 %reduce-scatter.2.cloned.1.call-done = bf16[144,2048]{1,0:T(8,128)(2,1)} async-done(((bf16[2304,2048]{1,0:T(8,128)(2,1)}), bf16[144,2048]{1,0:T(8,128)(2,1)}) %reduce-scatter.2.cloned.1.call-update) | async-done | bytes 589840 | tf_op jit(solution)/shard_map/reduce_scatter | solution.py:97
  231.5 2.3 reshape.89
  233.8 7.2 %all-to-all-start.2 = ((bf16[16,9,2048]{2,1,0:T(8,128)(2,1)}), bf16[16,9,2048]{2,1,0:T(8,128)(2,1)S(1)}, u32[]{:S(2)}, u32[]{:S(2)}) async-start(bf16[16,9,2048]{2,1,0:T(8,128)(2,1)} %reshape.89), calls=%async_computation.3 | async-start | bytes 2097152 | tf_op jit(solution)/shard_map/all_to_all | solution.py:103
  241.0 0.1 copy.24
  241.1 36.6 %all-gather.6.cloned.1.call-done = bf16[1024,2048]{1,0:T(8,128)(2,1)} async-done(((bf16[64,2048]{1,0:T(8,128)(2,1)}), bf16[1024,2048]{1,0:T(8,128)(2,1)}) %all-gather.6.cloned.1.call-update) | async-done | bytes 4194320 | tf_op jit(solution)/shard_map/all_gather | solution.py:63
  277.7 3.7 %convolution_convert_fusion.3 = bf16[128,2048]{1,0:T(8,128)(2,1)} fusion(bf16[128,1024]{0,1:T(8,128)(2,1)S(1)} %bitcast.36, bf16[1024,2048]{1,0:T(8,128)(2,1)} %all-gather.6.cloned.1.call-done), kind=kOutput, calls=%fused_computation.6 | convolution fusion | flops 537133056 | bytes 4980736 | tf_op jit(solution)/shard_map/dot_general | solution.py:61
  281.4 0.3 reshape.90
  281.6 0.9 gather_fusion
  282.6 0.7 reshape.91
  283.2 2.2 multiply_reduce_fusion
  (29 shorter events, 0.1 us)
Async XLA Ops:
  7.2 99.3 %copy-start = (bf16[1,256,2048]{2,1,0:T(8,128)(2,1)S(1)}, bf16[1,256,2048]{2,1,0:T(8,128)(2,1)}, u32[]{:S(2)}) copy-start(bf16[1,256,2048]{2,1,0:T(8,128)(2,1)} %param.27) | copy-start | bytes 3145732
  7.2 91.6 %all-gather.8.cloned.1.call-start = ((), (), s32[]{:S(2)}) async-start(), calls=%async_computation.6 | async-start | bytes 10027008 | tf_op jit(solution)/shard_map/all_gather | solution.py:93
  12.4 24.6 %copy-start.3 = (bf16[2048]{0:T(1024)(128)(2,1)S(1)}, bf16[2048]{0:T(1024)(128)(2,1)}, u32[]{:S(2)}) copy-start(bf16[2048]{0:T(1024)(128)(2,1)} %param.15) | copy-start | bytes 12292
  35.8 1.2 copy-start.1
  36.9 61.8 %copy-start.5 = (bf16[1,2048,256]{2,1,0:T(8,128)(2,1)S(1)}, bf16[1,2048,256]{2,1,0:T(8,128)(2,1)}, u32[]{:S(2)}) copy-start(bf16[1,2048,256]{2,1,0:T(8,128)(2,1)} %param.25) | copy-start | bytes 3145732
  36.9 118.6 %all-gather.4.cloned.1.call-start = ((), (), s32[]{:S(2)}) async-start(), calls=%async_computation.4 | async-start | bytes 8912896 | tf_op jit(solution)/shard_map/all_gather | solution.py:40
  38.2 193.3 %reduce-scatter.2.cloned.1.call-start = ((), (), s32[]{:S(2)}) async-start(), calls=%async_computation.7 | async-start | bytes 10027008 | tf_op jit(solution)/shard_map/reduce_scatter | solution.py:97
  121.4 0.7 copy-start.4
  121.4 34.2 %copy-start.6 = (bf16[2048,64]{0,1:T(8,128)(2,1)S(1)}, bf16[2048,64]{0,1:T(8,128)(2,1)}, u32[]{:S(2)}) copy-start(bf16[2048,64]{0,1:T(8,128)(2,1)} %param.18) | copy-start | bytes 786436
  121.4 34.2 %copy-start.7 = (bf16[2048,64]{0,1:T(8,128)(2,1)S(1)}, bf16[2048,64]{0,1:T(8,128)(2,1)}, u32[]{:S(2)}) copy-start(bf16[2048,64]{0,1:T(8,128)(2,1)} %param.17) | copy-start | bytes 786436
  121.4 34.2 %copy-start.8 = (bf16[2048,64]{0,1:T(8,128)(2,1)S(1)}, bf16[2048,64]{0,1:T(8,128)(2,1)}, u32[]{:S(2)}) copy-start(bf16[2048,64]{0,1:T(8,128)(2,1)} %param.16) | copy-start | bytes 786436
  121.4 156.2 %all-gather.6.cloned.1.call-start = ((), (), s32[]{:S(2)}) async-start(), calls=%async_computation.5 | async-start | bytes 4456448 | tf_op jit(solution)/shard_map/all_gather | solution.py:63
  122.1 50.5 %copy-start.2 = (f32[64,2]{0,1:T(2,128)S(1)}, f32[64,2]{0,1:T(2,128)}, u32[]{:S(2)}) copy-start(f32[64,2]{0,1:T(2,128)} %param.24) | copy-start | bytes 1540
  162.0 3.9 %collective-permute-start = (bf16[2,64]{0,1:T(8,128)(2,1)S(1)}, bf16[2,64]{0,1:T(8,128)(2,1)S(1)}, u32[]{:S(2)}, u32[]{:S(2)}) collective-permute-start(bf16[2,64]{0,1:T(8,128)(2,1)S(1)} %slice.41), channel_id=1, source_target_pairs={{0,16},{16,32},{32,48},{48,64},{64,80},{80,96},{96,112},{112,128},... | collective-permute-start | bytes 776 | tf_op jit(solution)/shard_map/ppermute | solution.py:12
  167.0 66.8 %all-to-all-start = ((bf16[16,128,64]{1,2,0:T(8,128)(2,1)}), bf16[16,128,64]{1,2,0:T(8,128)(2,1)S(1)}, u32[]{:S(2)}, u32[]{:S(2)}) async-start(bf16[16,128,64]{1,2,0:T(8,128)(2,1)} %copy_bitcast_fusion), calls=%async_computation | async-start | bytes 524288 | tf_op jit(solution)/shard_map/all_to_all | solution.py:60
  233.8 47.6 %all-to-all-start.2 = ((bf16[16,9,2048]{2,1,0:T(8,128)(2,1)}), bf16[16,9,2048]{2,1,0:T(8,128)(2,1)S(1)}, u32[]{:S(2)}, u32[]{:S(2)}) async-start(bf16[16,9,2048]{2,1,0:T(8,128)(2,1)} %reshape.89), calls=%async_computation.3 | async-start | bytes 2097152 | tf_op jit(solution)/shard_map/all_to_all | solution.py:103
Sparse Core Ops, SparseCore 0:
  37.0 61.6 all-gather.7
  101.1 54.3 all-gather.3
  158.1 73.3 reduce-scatter.1
  233.2 44.4 all-gather.5
where the time goes:
time: 293 us; the launch traced here: 292 us
  waiting for transfers between devices  191 us (65%)
  matrix products  34 us (12%)
  blocking collectives  23.4 us (8%)
  starting transfers between devices  15.8 us (5%)
  between operations  14 us (5%)
  local copies, waits for them, and re-layouts  7.02 us (2%)
  other arithmetic  6.89 us (2%)
    all_gather x1, waiting for transfers between devices, shards(): portion = lax.all_gather(arrived_rows, 'tp', axis=0, tiled=True)  60.5 us
    reduce_scatter x1, waiting for transfers between devices, shards(): lax.psum_scatter(jnp.dot(hidden, w_down, preferred_element_type=jnp.float...  58.9 us
    all_gather x1, waiting for transfers between devices, shards(): lax.all_gather(out_proj, 'tp', axis=0, tiled=True)  36.6 us
    all_gather x1, waiting for transfers between devices, shards(): lax.all_gather(normed, 'tp', axis=0, tiled=True)  33.5 us
    all_to_all x1, blocking collectives, shards(): lax.all_to_all(outgoing.reshape(experts, capacity, width_model), 'ep', sp...  23.4 us
    dot_general x1, matrix products, shards(): jnp.dot(hidden, w_down, preferred_element_type=jnp.float32)  14.9 us
    dot_general x1, matrix products, shards(): gate_value = jnp.dot(portion, w_gate, preferred_element_type=jnp.float32)  7.71 us
    all_to_all x1, starting transfers between devices, shards(): lax.all_to_all(summed.reshape(experts, capacity, width_model), 'ep', spli...  7.19 us
  transfers between devices with their start and end apart: 7, of which 5 were waited for; matrix products, arithmetic and copies ran while one was open for 13% of the time, Pallas kernels for 0%

commit v1 on v0

--- a/solution.py
+++ b/solution.py
@@ -58,10 +58,29 @@
         )
     carried = (out_gate.astype(jnp.float32) * convolved).astype(jnp.bfloat16)
     token_major = lax.all_to_all(carried, "tp", split_axis=0, concat_axis=1, tiled=True)
+
+    def table_touch(w_in):
+        n_dev_all = lax.axis_size("tp")
+        cards = []
+        for c in range(n_dev_all):
+            cards.append((c, (c + 1) % n_dev_all))
+        pile = []
+        for c in range(n_dev_all):
+            pile.append((c, (c - 1) % n_dev_all))
+        moved, top = ([w_in], [w_in])
+        for _ in range(n_dev_all // 2):
+            mixed_arr = lax.ppermute(moved[-1], "tp", cards)
+            moved.append(mixed_arr)
+        for _ in range((n_dev_all - 1) // 2):
+            top.append(lax.ppermute(top[-1], "tp", pile))
+        return jnp.roll(
+            jnp.concatenate([*moved[::-1], *top[1:]], axis=0),
+            (lax.axis_index("tp") - n_dev_all // 2) * w_in.shape[0],
+            axis=0,
+        )
+
     mix_out = jnp.dot(
-        token_major,
-        lax.all_gather(out_proj, "tp", axis=0, tiled=True),
-        preferred_element_type=jnp.float32,
+        token_major, table_touch(out_proj), preferred_element_type=jnp.float32
     ).astype(jnp.bfloat16)
     moe_normed = scaled_norm(moe_tokens, moe_gain)
     experts = expert_gate.shape[0] * lax.axis_size("ep")

time: 293 us -> 298 us (1.017)
  waiting for transfers between devices: 191 us -> 105 us
  starting transfers between devices: 15.8 us -> 68.9 us
  local copies, waits for them, and re-layouts: 7.02 us -> 41.5 us
    reduce_scatter x1, waiting for transfers between devices: 58.9 us -> 0.01 us  [shards(): lax.psum_scatter(jnp.dot(hidden, w_down, preferred_element_type=jnp.float...]
    ppermute x0 -> x15, starting transfers between devices: none -> 44.5 us  [the longest x7 32.7 us: table_touch(): top.append(lax.ppermute(top[-1], 'tp', pile))]
    all_gather x1 -> x0, waiting for transfers between devices: 36.6 us -> none  [shards(): lax.all_gather(out_proj, 'tp', axis=0, tiled=True)]
    unnamed x19 -> x50, local copies, waits for them, and re-layouts: 0.94 us -> 34.7 us
    all_gather x1, waiting for transfers between devices: 33.5 us -> 0.01 us  [shards(): lax.all_gather(normed, 'tp', axis=0, tiled=True)]
    ppermute x0 -> x15, waiting for transfers between devices: none -> 27.2 us  [the longest x8 26.3 us: table_touch(): mixed_arr = lax.ppermute(moved[-1], 'tp', cards)]
    all_to_all x1, waiting for transfers between devices: 0.01 us -> 14 us  [shards(): lax.all_to_all(summed.reshape(experts, capacity, width_model), 'ep', spli...]
    all_to_all x1, starting transfers between devices: 5.41 us -> 14 us  [shards(): lax.all_to_all(carried, 'tp', split_axis=0, concat_axis=1, tiled=True)]
  transfers between devices with their start and end apart: 7 -> 21, of which waited for: 5 -> 14; matrix products, arithmetic and copies ran while one was open for 13% -> 25% of each run, Pallas kernels for 0% -> 0%
where the time goes in v1:
time: 298 us; the launch traced here: 297 us
  waiting for transfers between devices  105 us (35%)
  starting transfers between devices  68.9 us (23%)
  local copies, waits for them, and re-layouts  41.5 us (14%)
  matrix products  34.2 us (11%)
  blocking collectives  23.4 us (8%)
  between operations  14 us (5%)
  other arithmetic  9.65 us (3%)
    all_gather x1, waiting for transfers between devices, shards(): portion = lax.all_gather(arrived_rows, 'tp', axis=0, tiled=True)  57.7 us
    unnamed x50, local copies, waits for them, and re-layouts  34.7 us
    ppermute x7, starting transfers between devices, table_touch(): top.append(lax.ppermute(top[-1], 'tp', pile))  32.7 us
    ppermute x8, waiting for transfers between devices, table_touch(): mixed_arr = lax.ppermute(moved[-1], 'tp', cards)  26.3 us
    all_to_all x1, blocking collectives, shards(): lax.all_to_all(outgoing.reshape(experts, capacity, width_model), 'ep', sp...  23.4 us
    dot_general x1, matrix products, shards(): jnp.dot(hidden, w_down, preferred_element_type=jnp.float32)  14.6 us
    all_to_all x1, waiting for transfers between devices, shards(): lax.all_to_all(summed.reshape(experts, capacity, width_model), 'ep', spli...  14 us
    all_to_all x1, starting transfers between devices, shards(): lax.all_to_all(carried, 'tp', split_axis=0, concat_axis=1, tiled=True)  14 us
  transfers between devices with their start and end apart: 21, of which 14 were waited for; matrix products, arithmetic and copies ran while one was open for 25% of the time, Pallas kernels for 0%

profile of v1, /device:TPU:1, one launch (start us, length us, event | category | flops | bytes accessed | tf_op | source)
XLA Modules:
  0.0 297.0 jit_solution(3866462380588941624)
XLA Ops:
  9.7 1.1 fusion.20
  10.8 1.3 convolution_convert_fusion.2
  12.4 23.4 %all_to_all.29 = bf16[16,9,2048]{2,1,0:T(8,128)(2,1)S(1)} all-to-all(bf16[16,9,2048]{2,1,0:T(8,128)(2,1)S(1)} %reshape.87), channel_id=1, replica_groups=mesh['ep'=16,'tp'=16] {'ep'}, dimensions={0} | all-to-all | bytes 1179648 | tf_op jit(solution)/shard_map/all_to_all | solution.py:101
  35.8 1.1 reshape.88
  37.7 1.2 fusion.7
  38.9 2.0 fusion.9
  41.0 57.7 %all-gather.5.cloned.1.call-done = bf16[2304,2048]{1,0:T(8,128)(2,1)} async-done(((bf16[144,2048]{1,0:T(8,128)(2,1)}), bf16[2304,2048]{1,0:T(8,128)(2,1)}) %all-gather.5.cloned.1.call-update) | async-done | bytes 9437200 | tf_op jit(solution)/shard_map/all_gather | solution.py:112
  98.7 8.0 %fusion.13 = f32[2304,256]{1,0:T(8,128)} fusion(bf16[2304,2048]{1,0:T(8,128)(2,1)} %all-gather.5.cloned.1.call-done, bf16[1,2048,256]{2,1,0:T(8,128)(2,1)} %param.25), kind=kOutput, calls=%fused_computation.17 | convolution fusion | flops 2415919104 | bytes 12845056 | tf_op jit(solution)/shard_map/dot_general | solution.py:113
  106.7 14.6 %convolution_convert_fusion = bf16[2304,2048]{1,0:T(8,128)(2,1)} fusion(bf16[2304,2048]{1,0:T(8,128)(2,1)} %all-gather.5.cloned.1.call-done, f32[2304,256]{1,0:T(8,128)} %fusion.13, bf16[1,256,2048]{2,1,0:T(8,128)(2,1)S(1)} %copy-done, bf16[1,2048,256]{2,1,0:T(8,128)(2,1)S(1)} %copy-done.8), kind=kOutput, calls=%fused_computation.1 | convolution fusion | flops 4840095744 | bytes 23330816 | tf_op jit(solution)/shard_map/dot_general | solution.py:117
  122.3 8.9 %collective-permute-done.1 = bf16[64,2048]{1,0:T(8,128)(2,1)S(1)} collective-permute-done((bf16[64,2048]{1,0:T(8,128)(2,1)S(1)}, bf16[64,2048]{1,0:T(8,128)(2,1)S(1)}, u32[]{:S(2)}, u32[]{:S(2)}) %collective-permute-start.1) | collective-permute-done | bytes 262176 | tf_op jit(solution)/shard_map/ppermute | solution.py:72
  131.2 2.5 collective-permute-start.2
  133.6 1.7 collective-permute-start.9
  135.3 7.4 %collective-permute-done.2 = bf16[64,2048]{1,0:T(8,128)(2,1)S(1)} collective-permute-done((bf16[64,2048]{1,0:T(8,128)(2,1)S(1)}, bf16[64,2048]{1,0:T(8,128)(2,1)S(1)}, u32[]{:S(2)}, u32[]{:S(2)}) %collective-permute-start.2) | collective-permute-done | bytes 262176 | tf_op jit(solution)/shard_map/ppermute | solution.py:72
  142.7 2.5 collective-permute-start.3
  145.2 2.9 collective-permute-start.10
  148.1 6.2 %collective-permute-done.3 = bf16[64,2048]{1,0:T(8,128)(2,1)S(1)} collective-permute-done((bf16[64,2048]{1,0:T(8,128)(2,1)S(1)}, bf16[64,2048]{1,0:T(8,128)(2,1)S(1)}, u32[]{:S(2)}, u32[]{:S(2)}) %collective-permute-start.3) | collective-permute-done | bytes 262176 | tf_op jit(solution)/shard_map/ppermute | solution.py:72
  154.2 2.5 collective-permute-start.4
  156.9 3.9 %collective-permute-start.11 = (bf16[64,2048]{1,0:T(8,128)(2,1)S(1)}, bf16[64,2048]{1,0:T(8,128)(2,1)S(1)}, u32[]{:S(2)}, u32[]{:S(2)}) collective-permute-start(bf16[64,2048]{1,0:T(8,128)(2,1)S(1)} %collective-permute-done.10), channel_id=1, source_target_pairs={{0,15},{1,0},{2,1},{3,2},{4,3},{5,4},{6,5},{7,6},{8,7},{9,8},{10,9... | collective-permute-start | bytes 786440 | tf_op jit(solution)/shard_map/ppermute | solution.py:75
  160.8 1.0 collective-permute-done.4
  161.8 2.4 collective-permute-start.5
  164.3 3.6 %collective-permute-start.12 = (bf16[64,2048]{1,0:T(8,128)(2,1)S(1)}, bf16[64,2048]{1,0:T(8,128)(2,1)S(1)}, u32[]{:S(2)}, u32[]{:S(2)}) collective-permute-start(bf16[64,2048]{1,0:T(8,128)(2,1)S(1)} %collective-permute-done.11), channel_id=1, source_target_pairs={{0,15},{1,0},{2,1},{3,2},{4,3},{5,4},{6,5},{7,6},{8,7},{9,8},{10,9... | collective-permute-start | bytes 786440 | tf_op jit(solution)/shard_map/ppermute | solution.py:75
  167.8 1.1 collective-permute-done.5
  169.0 1.2 collective-permute-start.6
  170.4 4.8 %collective-permute-start.13 = (bf16[64,2048]{1,0:T(8,128)(2,1)S(1)}, bf16[64,2048]{1,0:T(8,128)(2,1)}, u32[]{:S(2)}, u32[]{:S(2)}) collective-permute-start(bf16[64,2048]{1,0:T(8,128)(2,1)S(1)} %collective-permute-done.12), channel_id=1, source_target_pairs={{0,15},{1,0},{2,1},{3,2},{4,3},{5,4},{6,5},{7,6},{8,7},{9,8},{10,9... | collective-permute-start | bytes 786440 | tf_op jit(solution)/shard_map/ppermute | solution.py:75
  175.1 1.2 collective-permute-done.6
  176.4 8.0 %collective-permute-start.14 = (bf16[64,2048]{1,0:T(8,128)(2,1)}, bf16[64,2048]{1,0:T(8,128)(2,1)S(1)}, u32[]{:S(2)}, u32[]{:S(2)}) collective-permute-start(bf16[64,2048]{1,0:T(8,128)(2,1)} %collective-permute-done.13), channel_id=1, source_target_pairs={{0,15},{1,0},{2,1},{3,2},{4,3},{5,4},{6,5},{7,6},{8,7},{9,8},{10,9... | collective-permute-start | bytes 786440 | tf_op jit(solution)/shard_map/ppermute | solution.py:75
  185.8 7.9 %collective-permute-start.15 = (bf16[64,2048]{1,0:T(8,128)(2,1)S(1)}, bf16[64,2048]{1,0:T(8,128)(2,1)S(1)}, u32[]{:S(2)}, u32[]{:S(2)}) collective-permute-start(bf16[64,2048]{1,0:T(8,128)(2,1)S(1)} %collective-permute-done.14), channel_id=1, source_target_pairs={{0,15},{1,0},{2,1},{3,2},{4,3},{5,4},{6,5},{7,6},{8,7},{9,8},{10,9... | collective-permute-start | bytes 786440 | tf_op jit(solution)/shard_map/ppermute | solution.py:75
  194.4 1.7 constant_dynamic-update-slice_fusion.31
  196.0 1.7 constant_dynamic-update-slice_fusion.30
  197.7 1.7 constant_dynamic-update-slice_fusion.29
  199.4 1.7 constant_dynamic-update-slice_fusion.28
  201.1 1.7 constant_dynamic-update-slice_fusion.27
  208.5 1.7 constant_dynamic-update-slice_fusion.18
  211.7 1.7 constant_dynamic-update-slice_fusion.15
  213.4 1.7 constant_dynamic-update-slice_fusion.14
  215.0 1.7 constant_dynamic-update-slice_fusion.13
  216.7 1.7 constant_dynamic-update-slice_fusion.12
  222.8 6.6 %convolution_convert_fusion.1 = bf16[2048,192]{0,1:T(8,128)(2,1)S(1)} fusion(bf16[2048,2048]{1,0:T(8,128)(2,1)} %all-gather.3.cloned.1.call-done, bf16[2048,64]{0,1:T(8,128)(2,1)} %param.18, bf16[2048,64]{0,1:T(8,128)(2,1)} %param.17, bf16[2048,64]{0,1:T(8,128)(2,1)} %param.16), kind=kOutput, calls=%fused_computation.6 | convolution fusion | flops 1613365248 | bytes 9961472 | tf_op jit(solution)/shard_map/dot_general | solution.py:39
  229.5 3.0 %collective-permute-start = (bf16[2,64]{0,1:T(8,128)(2,1)S(1)}, bf16[2,64]{0,1:T(8,128)(2,1)S(1)}, u32[]{:S(2)}, u32[]{:S(2)}) collective-permute-start(bf16[2,64]{0,1:T(8,128)(2,1)S(1)} %slice.41), channel_id=1, source_target_pairs={{0,16},{16,32},{32,48},{48,64},{64,80},{80,96},{96,112},{112,128},... | collective-permute-start | bytes 776 | tf_op jit(solution)/shard_map/ppermute | solution.py:12
  233.4 1.0 copy_bitcast_fusion
  234.4 14.0 %all-to-all-start = ((bf16[16,128,64]{1,2,0:T(8,128)(2,1)}), bf16[16,128,64]{1,2,0:T(8,128)(2,1)S(1)}, u32[]{:S(2)}, u32[]{:S(2)}) async-start(bf16[16,128,64]{1,2,0:T(8,128)(2,1)} %copy_bitcast_fusion), calls=%async_computation | async-start | bytes 524288 | tf_op jit(solution)/shard_map/all_to_all | solution.py:60
  249.7 1.7 constant_dynamic-update-slice_fusion.2
  251.4 2.3 reshape.89
  253.7 6.2 %all-to-all-done = bf16[16,128,64]{1,2,0:T(8,128)(2,1)S(1)} async-done(((bf16[16,128,64]{1,2,0:T(8,128)(2,1)}), bf16[16,128,64]{1,2,0:T(8,128)(2,1)S(1)}, u32[]{:S(2)}, u32[]{:S(2)}) %all-to-all-start) | async-done | bytes 262176 | tf_op jit(solution)/shard_map/all_to_all | solution.py:60
  259.9 7.3 %all-to-all-start.2 = ((bf16[16,9,2048]{2,1,0:T(8,128)(2,1)}), bf16[16,9,2048]{2,1,0:T(8,128)(2,1)S(1)}, u32[]{:S(2)}, u32[]{:S(2)}) async-start(bf16[16,9,2048]{2,1,0:T(8,128)(2,1)} %reshape.89), calls=%async_computation.3 | async-start | bytes 2097152 | tf_op jit(solution)/shard_map/all_to_all | solution.py:122
  268.7 3.7 %fusion.3 = bf16[128,2048]{1,0:T(8,128)(2,1)} fusion(bf16[128,1024]{0,1:T(8,128)(2,1)S(1)} %bitcast.35, bf16[2048,2048]{1,0:T(8,128)(2,1)} %constant_dynamic-update-slice_fusion, s32[]{:T(128)S(6)} %select_n.24), kind=kOutput, calls=%fused_computation.8 | convolution fusion | flops 537133056 | bytes 4980740 | tf_op jit(solution)/shard_map/dot_general | solution.py:82
  272.4 14.0 %all-to-all-done.2 = bf16[16,9,2048]{2,1,0:T(8,128)(2,1)S(1)} async-done(((bf16[16,9,2048]{2,1,0:T(8,128)(2,1)}), bf16[16,9,2048]{2,1,0:T(8,128)(2,1)S(1)}, u32[]{:S(2)}, u32[]{:S(2)}) %all-to-all-start.2) | async-done | bytes 589856 | tf_op jit(solution)/shard_map/all_to_all | solution.py:122
  288.3 2.2 multiply_reduce_fusion
  (88 shorter events, 24.3 us)
Async XLA Ops:
  7.2 99.5 %copy-start = (bf16[1,256,2048]{2,1,0:T(8,128)(2,1)S(1)}, bf16[1,256,2048]{2,1,0:T(8,128)(2,1)}, u32[]{:S(2)}) copy-start(bf16[1,256,2048]{2,1,0:T(8,128)(2,1)} %param.27) | copy-start | bytes 3145732
  7.2 91.5 %all-gather.5.cloned.1.call-start = ((), (), s32[]{:S(2)}) async-start(), calls=%async_computation.5 | async-start | bytes 10027008 | tf_op jit(solution)/shard_map/all_gather | solution.py:112
  36.9 185.9 %all-gather.3.cloned.1.call-start = ((), (), s32[]{:S(2)}) async-start(), calls=%async_computation.4 | async-start | bytes 8912896 | tf_op jit(solution)/shard_map/all_gather | solution.py:40
  40.9 65.7 %copy-start.8 = (bf16[1,2048,256]{2,1,0:T(8,128)(2,1)S(1)}, bf16[1,2048,256]{2,1,0:T(8,128)(2,1)}, u32[]{:S(2)}) copy-start(bf16[1,2048,256]{2,1,0:T(8,128)(2,1)} %param.26) | copy-start | bytes 3145732
  41.0 210.4 %reduce-scatter.2.cloned.1.call-start = ((), (), s32[]{:S(2)}) async-start(), calls=%async_computation.6 | async-start | bytes 10027008 | tf_op jit(solution)/shard_map/reduce_scatter | solution.py:116
  121.3 1.0 copy-start.1
  121.3 49.0 %copy-start.6 = (f32[64,2]{0,1:T(2,128)S(1)}, f32[64,2]{0,1:T(2,128)}, u32[]{:S(2)}) copy-start(f32[64,2]{0,1:T(2,128)} %param.24) | copy-start | bytes 1540
  121.3 63.8 %copy-start.7 = (bf16[3,64]{1,0:T(4,128)(2,1)S(1)}, bf16[3,64]{1,0:T(4,128)(2,1)}, u32[]{:S(2)}) copy-start(bf16[3,64]{1,0:T(4,128)(2,1)} %param.19) | copy-start | bytes 1156
  122.3 8.9 %collective-permute-start.1 = (bf16[64,2048]{1,0:T(8,128)(2,1)S(1)}, bf16[64,2048]{1,0:T(8,128)(2,1)S(1)}, u32[]{:S(2)}, u32[]{:S(2)}) collective-permute-start(bf16[64,2048]{1,0:T(8,128)(2,1)S(1)} %copy-done.1), channel_id=1, source_target_pairs={{0,1},{1,2},{2,3},{3,4},{4,5},{5,6},{6,7},{7,8},{8,9},{9,10},{10,1... | collective-permute-start | bytes 786440 | tf_op jit(solution)/shard_map/ppermute | solution.py:72
  131.2 11.5 %collective-permute-start.2 = (bf16[64,2048]{1,0:T(8,128)(2,1)S(1)}, bf16[64,2048]{1,0:T(8,128)(2,1)S(1)}, u32[]{:S(2)}, u32[]{:S(2)}) collective-permute-start(bf16[64,2048]{1,0:T(8,128)(2,1)S(1)} %collective-permute-done.1), channel_id=1, source_target_pairs={{0,1},{1,2},{2,3},{3,4},{4,5},{5,6},{6,7},{7,8},{8,9},{9,10},{10,1... | collective-permute-start | bytes 786440 | tf_op jit(solution)/shard_map/ppermute | solution.py:72
  133.6 11.5 %collective-permute-start.9 = (bf16[64,2048]{1,0:T(8,128)(2,1)S(1)}, bf16[64,2048]{1,0:T(8,128)(2,1)S(1)}, u32[]{:S(2)}, u32[]{:S(2)}) collective-permute-start(bf16[64,2048]{1,0:T(8,128)(2,1)S(1)} %copy-done.1), channel_id=1, source_target_pairs={{0,15},{1,0},{2,1},{3,2},{4,3},{5,4},{6,5},{7,6},{8,7},{9,8},{10,9... | collective-permute-start | bytes 786440 | tf_op jit(solution)/shard_map/ppermute | solution.py:75
  142.7 11.5 %collective-permute-start.3 = (bf16[64,2048]{1,0:T(8,128)(2,1)S(1)}, bf16[64,2048]{1,0:T(8,128)(2,1)S(1)}, u32[]{:S(2)}, u32[]{:S(2)}) collective-permute-start(bf16[64,2048]{1,0:T(8,128)(2,1)S(1)} %collective-permute-done.2), channel_id=1, source_target_pairs={{0,1},{1,2},{2,3},{3,4},{4,5},{5,6},{6,7},{7,8},{8,9},{9,10},{10,1... | collective-permute-start | bytes 786440 | tf_op jit(solution)/shard_map/ppermute | solution.py:72
  145.2 11.7 %collective-permute-start.10 = (bf16[64,2048]{1,0:T(8,128)(2,1)S(1)}, bf16[64,2048]{1,0:T(8,128)(2,1)S(1)}, u32[]{:S(2)}, u32[]{:S(2)}) collective-permute-start(bf16[64,2048]{1,0:T(8,128)(2,1)S(1)} %collective-permute-done.9), channel_id=1, source_target_pairs={{0,15},{1,0},{2,1},{3,2},{4,3},{5,4},{6,5},{7,6},{8,7},{9,8},{10,9... | collective-permute-start | bytes 786440 | tf_op jit(solution)/shard_map/ppermute | solution.py:75
  154.2 7.6 %collective-permute-start.4 = (bf16[64,2048]{1,0:T(8,128)(2,1)S(1)}, bf16[64,2048]{1,0:T(8,128)(2,1)S(1)}, u32[]{:S(2)}, u32[]{:S(2)}) collective-permute-start(bf16[64,2048]{1,0:T(8,128)(2,1)S(1)} %collective-permute-done.3), channel_id=1, source_target_pairs={{0,1},{1,2},{2,3},{3,4},{4,5},{5,6},{6,7},{7,8},{8,9},{9,10},{10,1... | collective-permute-start | bytes 786440 | tf_op jit(solution)/shard_map/ppermute | solution.py:72
  156.9 7.4 %collective-permute-start.11 = (bf16[64,2048]{1,0:T(8,128)(2,1)S(1)}, bf16[64,2048]{1,0:T(8,128)(2,1)S(1)}, u32[]{:S(2)}, u32[]{:S(2)}) collective-permute-start(bf16[64,2048]{1,0:T(8,128)(2,1)S(1)} %collective-permute-done.10), channel_id=1, source_target_pairs={{0,15},{1,0},{2,1},{3,2},{4,3},{5,4},{6,5},{7,6},{8,7},{9,8},{10,9... | collective-permute-start | bytes 786440 | tf_op jit(solution)/shard_map/ppermute | solution.py:75
  161.8 14.5 %copy-start.2 = (bf16[64,2048]{1,0:T(8,128)(2,1)}, bf16[64,2048]{1,0:T(8,128)(2,1)S(1)}, u32[]{:S(2)}) copy-start(bf16[64,2048]{1,0:T(8,128)(2,1)S(1)} %collective-permute-done.4) | copy-start | bytes 786436
  161.8 7.1 %collective-permute-start.5 = (bf16[64,2048]{1,0:T(8,128)(2,1)S(1)}, bf16[64,2048]{1,0:T(8,128)(2,1)}, u32[]{:S(2)}, u32[]{:S(2)}) collective-permute-start(bf16[64,2048]{1,0:T(8,128)(2,1)S(1)} %collective-permute-done.4), channel_id=1, source_target_pairs={{0,1},{1,2},{2,3},{3,4},{4,5},{5,6},{6,7},{7,8},{8,9},{9,10},{10,1... | collective-permute-start | bytes 786440 | tf_op jit(solution)/shard_map/ppermute | solution.py:72
  164.3 6.1 %collective-permute-start.12 = (bf16[64,2048]{1,0:T(8,128)(2,1)S(1)}, bf16[64,2048]{1,0:T(8,128)(2,1)S(1)}, u32[]{:S(2)}, u32[]{:S(2)}) collective-permute-start(bf16[64,2048]{1,0:T(8,128)(2,1)S(1)} %collective-permute-done.11), channel_id=1, source_target_pairs={{0,15},{1,0},{2,1},{3,2},{4,3},{5,4},{6,5},{7,6},{8,7},{9,8},{10,9... | collective-permute-start | bytes 786440 | tf_op jit(solution)/shard_map/ppermute | solution.py:75
  169.0 7.3 %collective-permute-start.6 = (bf16[64,2048]{1,0:T(8,128)(2,1)}, bf16[64,2048]{1,0:T(8,128)(2,1)}, u32[]{:S(2)}, u32[]{:S(2)}) collective-permute-start(bf16[64,2048]{1,0:T(8,128)(2,1)} %collective-permute-done.5), channel_id=1, source_target_pairs={{0,1},{1,2},{2,3},{3,4},{4,5},{5,6},{6,7},{7,8},{8,9},{9,10},{10,1... | collective-permute-start | bytes 786440 | tf_op jit(solution)/shard_map/ppermute | solution.py:72
  170.4 6.1 %collective-permute-start.13 = (bf16[64,2048]{1,0:T(8,128)(2,1)S(1)}, bf16[64,2048]{1,0:T(8,128)(2,1)}, u32[]{:S(2)}, u32[]{:S(2)}) collective-permute-start(bf16[64,2048]{1,0:T(8,128)(2,1)S(1)} %collective-permute-done.12), channel_id=1, source_target_pairs={{0,15},{1,0},{2,1},{3,2},{4,3},{5,4},{6,5},{7,6},{8,7},{9,8},{10,9... | collective-permute-start | bytes 786440 | tf_op jit(solution)/shard_map/ppermute | solution.py:75
  176.3 8.1 %collective-permute-start.7 = (bf16[64,2048]{1,0:T(8,128)(2,1)}, bf16[64,2048]{1,0:T(8,128)(2,1)}, u32[]{:S(2)}, u32[]{:S(2)}) collective-permute-start(bf16[64,2048]{1,0:T(8,128)(2,1)} %collective-permute-done.6), channel_id=1, source_target_pairs={{0,1},{1,2},{2,3},{3,4},{4,5},{5,6},{6,7},{7,8},{8,9},{9,10},{10,1... | collective-permute-start | bytes 786440 | tf_op jit(solution)/shard_map/ppermute | solution.py:72
  176.4 9.4 %collective-permute-start.14 = (bf16[64,2048]{1,0:T(8,128)(2,1)}, bf16[64,2048]{1,0:T(8,128)(2,1)S(1)}, u32[]{:S(2)}, u32[]{:S(2)}) collective-permute-start(bf16[64,2048]{1,0:T(8,128)(2,1)} %collective-permute-done.13), channel_id=1, source_target_pairs={{0,15},{1,0},{2,1},{3,2},{4,3},{5,4},{6,5},{7,6},{8,7},{9,8},{10,9... | collective-permute-start | bytes 786440 | tf_op jit(solution)/shard_map/ppermute | solution.py:75
  184.4 9.9 %collective-permute-start.8 = (bf16[64,2048]{1,0:T(8,128)(2,1)}, bf16[64,2048]{1,0:T(8,128)(2,1)}, u32[]{:S(2)}, u32[]{:S(2)}) collective-permute-start(bf16[64,2048]{1,0:T(8,128)(2,1)} %collective-permute-done.7), channel_id=1, source_target_pairs={{0,1},{1,2},{2,3},{3,4},{4,5},{5,6},{6,7},{7,8},{8,9},{9,10},{10,1... | collective-permute-start | bytes 786440 | tf_op jit(solution)/shard_map/ppermute | solution.py:72
  185.2 33.2 %copy-start.3 = (bf16[64,2048]{1,0:T(8,128)(2,1)S(1)}, bf16[64,2048]{1,0:T(8,128)(2,1)}, u32[]{:S(2)}) copy-start(bf16[64,2048]{1,0:T(8,128)(2,1)} %copy-done.2) | copy-start | bytes 786436
  185.8 25.1 %collective-permute-start.15 = (bf16[64,2048]{1,0:T(8,128)(2,1)S(1)}, bf16[64,2048]{1,0:T(8,128)(2,1)S(1)}, u32[]{:S(2)}, u32[]{:S(2)}) collective-permute-start(bf16[64,2048]{1,0:T(8,128)(2,1)S(1)} %collective-permute-done.14), channel_id=1, source_target_pairs={{0,15},{1,0},{2,1},{3,2},{4,3},{5,4},{6,5},{7,6},{8,7},{9,8},{10,9... | collective-permute-start | bytes 786440 | tf_op jit(solution)/shard_map/ppermute | solution.py:75
  210.9 11.1 %copy-start.4 = (bf16[64,2048]{1,0:T(8,128)(2,1)}, bf16[64,2048]{1,0:T(8,128)(2,1)S(1)}, u32[]{:S(2)}) copy-start(bf16[64,2048]{1,0:T(8,128)(2,1)S(1)} %collective-permute-done.15) | copy-start | bytes 786436
  222.8 45.2 %copy-start.5 = (bf16[64,2048]{1,0:T(8,128)(2,1)S(1)}, bf16[64,2048]{1,0:T(8,128)(2,1)}, u32[]{:S(2)}) copy-start(bf16[64,2048]{1,0:T(8,128)(2,1)} %copy-done.4) | copy-start | bytes 786436
  229.5 3.9 %collective-permute-start = (bf16[2,64]{0,1:T(8,128)(2,1)S(1)}, bf16[2,64]{0,1:T(8,128)(2,1)S(1)}, u32[]{:S(2)}, u32[]{:S(2)}) collective-permute-start(bf16[2,64]{0,1:T(8,128)(2,1)S(1)} %slice.41), channel_id=1, source_target_pairs={{0,16},{16,32},{32,48},{48,64},{64,80},{80,96},{96,112},{112,128},... | collective-permute-start | bytes 776 | tf_op jit(solution)/shard_map/ppermute | solution.py:12
  234.4 25.5 %all-to-all-start = ((bf16[16,128,64]{1,2,0:T(8,128)(2,1)}), bf16[16,128,64]{1,2,0:T(8,128)(2,1)S(1)}, u32[]{:S(2)}, u32[]{:S(2)}) async-start(bf16[16,128,64]{1,2,0:T(8,128)(2,1)} %copy_bitcast_fusion), calls=%async_computation | async-start | bytes 524288 | tf_op jit(solution)/shard_map/all_to_all | solution.py:60
  259.9 26.5 %all-to-all-start.2 = ((bf16[16,9,2048]{2,1,0:T(8,128)(2,1)}), bf16[16,9,2048]{2,1,0:T(8,128)(2,1)S(1)}, u32[]{:S(2)}, u32[]{:S(2)}) async-start(bf16[16,9,2048]{2,1,0:T(8,128)(2,1)} %reshape.89), calls=%async_computation.3 | async-start | bytes 2097152 | tf_op jit(solution)/shard_map/all_to_all | solution.py:122
Sparse Core Ops, SparseCore 0:
  37.0 61.6 all-gather.4
  101.1 62.8 all-gather.2
  166.5 74.3 reduce-scatter.1
